TPU v7x, 256 devices: a whole 4x4x8 slice. The times are simulated.
256 devices in a mesh: sp: 64 (over z, x, core), tp: 4 (over y).
Axes of the slice: x: 4, y: 4, z: 8, core: 2. Of those that a mesh axis runs over, the one named last changes fastest.
Arguments:
- stream: bfloat16 [8192, 2048], P(('sp', 'tp')), may hold values from -2.5 to 2.5
- recurrence_input: bfloat16 [8192, 2, 1024], P('sp', None, 'tp'), may hold values from -6 to 6
- output_gate_input: bfloat16 [8192, 2, 1024], P('sp', None, 'tp'), may hold values from -6 to 6
- convolution_taps: bfloat16 [4, 2, 1024], P(None, None, 'tp'), may hold values from -4 to 4
- first_group_gates: bfloat16 [2, 16, 64, 64], P(None, 'tp'), may hold values from -0.75 to 0.75
- second_group_gates: bfloat16 [2, 8, 128, 128], P(None, 'tp'), may hold values from -0.5 to 0.5
- channel_decay: float32 [2, 1024], P(None, 'tp'), may hold values from 4.7 to 13.6
- position_log_extra: float32 [8192, 2, 1024], P('sp', None, 'tp'), may hold values from -1.4 to 0, as said below
- recurrence_output_weight: bfloat16 [2, 1024, 2048], P(None, 'tp'), may hold values from -0.125 to 0.125
- first_norm_gain: float32 [2048], replicated, may hold values from 0.1 to 1.9
- first_norm_bias: float32 [2048], replicated, may hold values from -1.75 to 1.75
- routed_expert_index: int32 [8192, 4], P('sp'), may hold values from 0 to 63, all different within a row; in each aligned block of 32 rows (0 to 31, 32 to 63, ...) at most 2 rows name the same one
- routed_expert_weight: float32 [8192, 4], P('sp'), may hold values from 0.25 to 1
- routed_gate_weight: bfloat16 [64, 2048, 512], P('sp', None, 'tp'), may hold values from -0.125 to 0.125
- routed_up_weight: bfloat16 [64, 2048, 512], P('sp', None, 'tp'), may hold values from -0.125 to 0.125
- routed_down_weight: bfloat16 [64, 512, 2048], P('sp', 'tp'), may hold values from -0.25 to 0.25
- shared_gate_weight: bfloat16 [2048, 512], replicated, may hold values from -0.125 to 0.125
- shared_up_weight: bfloat16 [2048, 512], replicated, may hold values from -0.125 to 0.125
- shared_down_weight: bfloat16 [512, 2048], replicated, may hold values from -0.25 to 0.25
- second_norm_gain: float32 [2048], replicated, may hold values from 0.1 to 1.9
- second_norm_bias: float32 [2048], replicated, may hold values from -1.75 to 1.75
Outputs:
- result: bfloat16 [8192, 2048], P(('sp', 'tp'))
Inputs may be any that keep to these rules, and one draw needn't show every extreme that they name: `routed_expert_index`: each row names 4 different experts. In each aligned block of 32 rows no expert is named more than 2 times, and in some block an expert is named exactly 2 times. `position_log_extra`: every entry is negative.
All inputs are finite; a program needn't handle non-finite values.
Results may differ from a plain program's by a relative error of at most 0.015.
Values may be sent and summed in bfloat16 or wider, within the bound.
A program may use at most 64 MiB of HBM per device.

v0:
```python
import jax
import jax.numpy as jnp
from jax import lax
from jax.sharding import PartitionSpec as P

RESIDUAL_SCALE = 8.0**0.25
NORM_EPSILON = 1e-05


def copy_for_each(shard, axis):
    count = lax.axis_size(axis)
    return lax.all_to_all(
        jnp.broadcast_to(shard[None], (count, *shard.shape)), axis, 0, 0, tiled=True
    )


def all_in_one(shard, axis):
    leaves = jax.tree.leaves(shard)
    sequence = sorted(range(len(leaves)), key=lambda k: -leaves[k].size)
    width = (1, *leaves[sequence[0]].shape)[-1]
    lines = [
        jnp.pad(leaves[k].reshape(-1), (0, -leaves[k].size % width)).reshape(-1, width)
        for k in sequence
    ]
    both, at, found = (copy_for_each(jnp.concatenate(lines), axis), 0, {})
    for k, line in zip(sequence, lines):
        slab = both[:, at : at + len(line)].reshape(len(both), -1)
        found[k] = slab[:, : leaves[k].size].reshape(-1, *leaves[k].shape)
        at += len(line)
    numbers = iter(range(len(leaves)))
    return jax.tree.map(lambda _: found[next(numbers)], shard)


def joined_by_halves(pieces, combine):
    while len(jax.tree.leaves(pieces)[0]) > 1:
        pieces = jax.vmap(combine)(
            *(jax.tree.map(lambda part: part[side::2], pieces) for side in (0, 1))
        )
    return jax.tree.map(lambda part: part[0], pieces)


def entering(shard, axis, combine, identity):
    count, mine = (lax.axis_size(axis), lax.axis_index(axis))
    passed = jnp.arange(count) < mine

    def kept(part, zero, own):
        part = jnp.where(
            passed.reshape(-1, *(1 for _ in own.shape)), part, jnp.asarray(zero, own.dtype)
        )
        return part

    pieces = all_in_one(shard, axis)
    return joined_by_halves(jax.tree.map(kept, pieces, identity, shard), combine)


def shifted(shard, axis, by):
    count = lax.axis_size(axis)
    pairs = [(i, i + by) for i in range(count) if 0 <= i + by < count]
    return lax.ppermute(shard, axis, pairs)


def cut_along(shard, dim, count):
    dims = shard.shape
    pieces = shard.reshape(*dims[:dim], count, dims[dim] // count, *dims[dim + 1 :])
    return jnp.moveaxis(pieces, dim, 0)


def summed_on_arrival(shard, axis, dim):
    count = lax.axis_size(axis)
    pieces = lax.all_to_all(cut_along(shard, dim, count), axis, 0, 0, tiled=True)
    return jnp.sum(pieces.astype(jnp.float32), axis=0)


def layer_norm(values, gain_vec, bias_vec):
    row_mean = jnp.mean(values, axis=-1, keepdims=True)
    spread = jnp.mean(jnp.square(values - row_mean), axis=-1, keepdims=True)
    return (values - row_mean) * lax.rsqrt(spread + NORM_EPSILON) * gain_vec + bias_vec


def block_gates(conv_rows, weights, head_size):
    length = conv_rows.shape[0]
    head_rows = conv_rows.reshape(length, -1, head_size)
    pre_act = jnp.einsum("thc,ghcd->gthd", head_rows, weights, preferred_element_type=jnp.float32)
    gate_pair = jax.nn.sigmoid(pre_act).reshape(2, length, -1)
    return (gate_pair[0], gate_pair[1])


def chain_link(first_part, second_part):
    return (first_part[0] * second_part[0], second_part[0] * first_part[1] + second_part[1])


def carried(totals):
    unity = jnp.ones_like(totals[0])
    nought = jnp.zeros_like(totals[1])
    return entering(totals, "sp", chain_link, (unity, nought))[1]


def expert_terms(picked, letters, gate_w, up_w, down_w):
    gate_form = letters + "d,ldf->" + letters + "f"
    down_form = letters + "f,lfd->" + letters + "d"
    gated = jnp.einsum(gate_form, picked, gate_w, preferred_element_type=jnp.float32)
    lifted = jnp.einsum(gate_form, picked, up_w, preferred_element_type=jnp.float32)
    hidden = (jax.nn.silu(gated) * lifted).astype(jnp.bfloat16)
    return jnp.einsum(down_form, hidden, down_w, preferred_element_type=jnp.float32)


def shards(
    stream,
    recurrence_input,
    output_gate_input,
    convolution_taps,
    first_group_gates,
    second_group_gates,
    channel_decay,
    position_log_extra,
    recurrence_output_weight,
    first_norm_gain,
    first_norm_bias,
    routed_expert_index,
    routed_expert_weight,
    routed_gate_weight,
    routed_up_weight,
    routed_down_weight,
    shared_gate_weight,
    shared_up_weight,
    shared_down_weight,
    second_norm_gain,
    second_norm_bias,
):
    length = recurrence_input.shape[0]
    tap_count = convolution_taps.shape[0]
    border = shifted(recurrence_input[length - (tap_count - 1) :], "sp", 1)
    padded = jnp.concatenate([border, recurrence_input], axis=0).astype(jnp.float32)
    tap_weights = convolution_taps.astype(jnp.float32)
    summed = tap_weights[0] * padded[0:length]
    for offset in range(1, tap_count):
        summed = summed + tap_weights[offset] * padded[offset : offset + length]
    conv_rows = summed.astype(jnp.bfloat16)
    recur_a, input_a = block_gates(conv_rows[:, 0], first_group_gates, first_group_gates.shape[-1])
    recur_b, input_b = block_gates(
        conv_rows[:, 1], second_group_gates, second_group_gates.shape[-1]
    )
    recurrence_gate = jnp.stack([recur_a, recur_b], axis=1)
    input_gate = jnp.stack([input_a, input_b], axis=1)
    decay_logarithm = -8.0 * recurrence_gate * jax.nn.softplus(-channel_decay) + position_log_extra
    decay_rate = jnp.exp(decay_logarithm)
    driving = (
        jnp.sqrt(-jnp.expm1(2.0 * decay_logarithm)) * input_gate * conv_rows.astype(jnp.float32)
    )
    running = jnp.cumsum(decay_logarithm, axis=0)
    tail_sum = jnp.sum(jnp.exp(running[-1] - running) * driving, axis=0)
    incoming = carried((jnp.exp(running[-1]), tail_sum))
    opening = driving[:1] + decay_rate[:1] * incoming
    started = jnp.concatenate([opening, driving[1:]], axis=0)
    states = lax.associative_scan(chain_link, (decay_rate, started), axis=0)[1]
    branch_output = (jax.nn.gelu(output_gate_input.astype(jnp.float32)) * states).astype(
        jnp.bfloat16
    )
    tp_count = lax.axis_size("tp")
    quarter = length // tp_count
    mixed = summed_on_arrival(
        jnp.einsum(
            "tgc,gcd->td",
            branch_output,
            recurrence_output_weight,
            preferred_element_type=jnp.float32,
        ).astype(jnp.bfloat16),
        "tp",
        0,
    )
    normed = layer_norm(
        RESIDUAL_SCALE * stream.astype(jnp.float32) + mixed, first_norm_gain, first_norm_bias
    ).astype(jnp.bfloat16)
    width = normed.shape[1]
    top_count = routed_expert_index.shape[1]
    local_count = routed_gate_weight.shape[0]
    expert_count = local_count * lax.axis_size("sp")
    capacity = max(2, 5 * quarter * top_count // (4 * expert_count))
    block_ids = routed_expert_index.reshape(tp_count, quarter * top_count)
    onehot = (
        block_ids[:, :, None] == jnp.arange(expert_count, dtype=jnp.int32)[None, None, :]
    ).astype(jnp.int32)
    slot_ranks = jnp.sum((jnp.cumsum(onehot, axis=1) - onehot) * onehot, axis=2)
    own_index = lax.axis_index("tp")
    own_ids = lax.dynamic_index_in_dim(block_ids, own_index, 0, keepdims=False)
    own_ranks = lax.dynamic_index_in_dim(slot_ranks, own_index, 0, keepdims=False)
    blank_row = jnp.zeros((1, width), jnp.bfloat16)
    padded_rows = jnp.concatenate([normed, blank_row], axis=0)
    targets = own_ids * capacity + own_ranks
    sources = jnp.arange(quarter * top_count, dtype=jnp.int32) // top_count
    table = jnp.full((expert_count * capacity,), quarter, jnp.int32).at[targets].set(sources)
    outgoing = jnp.take(padded_rows, table, axis=0).reshape(expert_count, capacity, width)
    arrived = lax.all_to_all(outgoing, "sp", split_axis=0, concat_axis=0, tiled=True)
    slots = arrived.shape[1]
    fanned = lax.all_gather(arrived[None], "tp", axis=0, tiled=True)
    shaped = fanned.reshape(tp_count, -1, local_count, slots, width)
    partial_value = expert_terms(
        shaped, "xslc", routed_gate_weight, routed_up_weight, routed_down_weight
    )
    summed_rows = summed_on_arrival(partial_value.astype(jnp.bfloat16), "tp", 0)
    leaving = summed_rows.astype(jnp.bfloat16).reshape(-1, slots, width)
    returned = lax.all_to_all(leaving, "sp", split_axis=0, concat_axis=0, tiled=True)
    picked_rows = returned.reshape(expert_count * capacity, width)[own_ids * capacity + own_ranks]
    own_weights = lax.dynamic_slice_in_dim(routed_expert_weight, own_index * quarter, quarter, 0)
    routed = jnp.sum(
        own_weights[:, :, None]
        * picked_rows.reshape(quarter, top_count, width).astype(jnp.float32),
        axis=1,
    )
    shared_hidden = (
        jax.nn.silu(jnp.dot(normed, shared_gate_weight, preferred_element_type=jnp.float32))
        * jnp.dot(normed, shared_up_weight, preferred_element_type=jnp.float32)
    ).astype(jnp.bfloat16)
    shared_out = jnp.dot(shared_hidden, shared_down_weight, preferred_element_type=jnp.float32)
    final = layer_norm(
        RESIDUAL_SCALE * normed.astype(jnp.float32) + (shared_out + routed),
        second_norm_gain,
        second_norm_bias,
    )
    return final.astype(jnp.bfloat16)


def solution(mesh):
    in_specs = (
        P(("sp", "tp"), None),
        P("sp", None, "tp"),
        P("sp", None, "tp"),
        P(None, None, "tp"),
        P(None, "tp", None, None),
        P(None, "tp", None, None),
        P(None, "tp"),
        P("sp", None, "tp"),
        P(None, "tp", None),
        P(),
        P(),
        P("sp", None),
        P("sp", None),
        P("sp", None, "tp"),
        P("sp", None, "tp"),
        P("sp", "tp", None),
        P(),
        P(),
        P(),
        P(),
        P(),
    )
    out_specs = P(("sp", "tp"), None)
    return jax.shard_map(shards, mesh=mesh, in_specs=in_specs, out_specs=out_specs, check_vma=False)
```

profile of v0, /device:TPU:1, one launch (start us, length us, event | category | flops | bytes accessed | tf_op | source)
XLA Modules:
  0.0 205.7 jit_solution(793034132163294517)
XLA Ops:
  6.5 1.1 copy.130
  7.6 4.5 %collective-permute-start = (bf16[3,2,256]{2,0,1:T(4,128)(2,1)S(1)}, bf16[3,2,256]{2,0,1:T(4,128)(2,1)S(1)}, u32[]{:S(2)}, u32[]{:S(2)}) collective-permute-start(bf16[3,2,256]{2,0,1:T(4,128)(2,1)S(1)} %slice.395), channel_id=1, source_target_pairs={{0,4},{4,8},{8,12},{12,16},{16,20},{20,24},{24,28},{28,32},{32,36}... | collective-permute-start | bytes 9224 | tf_op jit(solution)/shard_map/ppermute | solution.py:59
  13.6 0.8 copy.147
  16.4 1.0 fusion.101
  19.6 1.2 fusion.52
  21.6 11.3 %all-to-all-start = ((f32[64,4,256]{2,1,0:T(4,128)}), f32[64,4,256]{2,1,0:T(4,128)S(1)}, u32[]{:S(2)}, u32[]{:S(2)}) async-start(f32[64,4,256]{2,1,0:T(4,128)} %broadcast_in_dim.61), calls=%async_computation | async-start | bytes 524288 | tf_op jit(solution)/shard_map/all_to_all | solution.py:12
  32.9 0.8 fusion.60
  34.0 0.9 select_reduce_fusion
  35.6 1.5 scatter_custom_fusion
  38.7 7.3 %all-to-all-done = f32[64,4,256]{2,1,0:T(4,128)S(1)} async-done(((f32[64,4,256]{2,1,0:T(4,128)}), f32[64,4,256]{2,1,0:T(4,128)S(1)}, u32[]{:S(2)}, u32[]{:S(2)}) %all-to-all-start) | async-done | bytes 262176 | tf_op jit(solution)/shard_map/all_to_all | solution.py:12
  47.5 0.9 fusion.109
  49.0 1.0 fusion.106
  51.7 1.3 fusion.1
  53.0 4.3 %all-to-all-start.1 = ((bf16[4,32,2048]{2,1,0:T(8,128)(2,1)}), bf16[4,32,2048]{2,1,0:T(8,128)(2,1)S(1)}, u32[]{:S(2)}, u32[]{:S(2)}) async-start(bf16[4,32,2048]{2,1,0:T(8,128)(2,1)} %bitcast.17), calls=%async_computation.1 | async-start | bytes 1048576 | tf_op jit(solution)/shard_map/all_to_all | solution.py:70
  57.5 8.8 %all-to-all-done.1 = bf16[4,32,2048]{2,1,0:T(8,128)(2,1)S(1)} async-done(((bf16[4,32,2048]{2,1,0:T(8,128)(2,1)}), bf16[4,32,2048]{2,1,0:T(8,128)(2,1)S(1)}, u32[]{:S(2)}, u32[]{:S(2)}) %all-to-all-start.1) | async-done | bytes 524320 | tf_op jit(solution)/shard_map/all_to_all | solution.py:70
  67.0 0.9 gather_fusion
  67.9 1.1 gather.10
  69.0 1.6 broadcast_select_fusion
  70.6 23.1 %all_to_all.25 = bf16[64,2,2048]{2,1,0:T(2,128)(2,1)S(1)} all-to-all(bf16[64,2,2048]{2,1,0:T(2,128)(2,1)S(1)} %broadcast_select_fusion), channel_id=1, replica_groups=mesh['sp'=64,'tp'=4] {'sp'}, dimensions={0} | all-to-all | bytes 1048576 | tf_op jit(solution)/shard_map/all_to_all | solution.py:193
  93.8 1.0 copy.148
  94.8 27.8 %all-gather.3.cloned.1.call-done = bf16[256,2,2048]{2,0,1:T(8,128)(2,1)} async-done(((bf16[64,2,2048]{2,0,1:T(8,128)(2,1)}), bf16[256,2,2048]{2,0,1:T(8,128)(2,1)}) %all-gather.3.cloned.1.call-update) | async-done | bytes 2097168 | tf_op jit(solution)/shard_map/all_gather | solution.py:195
  122.6 2.4 %fusion.7 = f32[4,64,1,2,128]{4,1,3,0,2:T(8,128)S(1)} fusion(bf16[4,64,2,2048]{3,1,0,2:T(8,128)(2,1)} %bitcast.118, bf16[1,2048,128]{2,1,0:T(8,128)(2,1)} %param.34), kind=kOutput, calls=%fused_computation.14 | convolution fusion | flops 268435456 | bytes 2883584 | tf_op jit(solution)/shard_map/xslcd,ldf->xslcf/dot_general | solution.py:101
  125.0 5.2 %fusion = bf16[4,1,64,1,2,2048]{5,2,4,3,1,0:T(8,128)(2,1)} fusion(bf16[4,64,2,2048]{3,1,0,2:T(8,128)(2,1)} %bitcast.119, bf16[1,128,2048]{2,1,0:T(8,128)(2,1)S(1)} %copy-done.2, bf16[1,2048,128]{2,1,0:T(8,128)(2,1)S(1)} %copy-done.3, f32[4,64,1,2,128]{4,1,3,0,2:T(8,128)S(1)} %fusion.7), kind=kOutput, calls=%fused_computation.4 | convolution fusion | flops 538312704 | bytes 5505024 | tf_op jit(solution)/shard_map/xslcf,lfd->xslcd/dot_general | solution.py:104
  130.2 28.9 %all_to_all.26 = bf16[4,1,64,1,2,2048]{5,2,4,3,1,0:T(8,128)(2,1)S(1)} all-to-all(bf16[4,1,64,1,2,2048]{5,2,4,3,1,0:T(8,128)(2,1)} %fusion), channel_id=1, replica_groups=mesh['sp'=64,'tp'=4] {'tp'}, dimensions={0} | all-to-all | bytes 4194304 | tf_op jit(solution)/shard_map/all_to_all | solution.py:70
  159.5 1.3 copy.153
  160.9 11.9 %all-to-all-start.4 = ((bf16[64,2,2048]{2,1,0:T(2,128)(2,1)}), bf16[64,2,2048]{2,1,0:T(2,128)(2,1)S(1)}, u32[]{:S(2)}, u32[]{:S(2)}) async-start(bf16[64,2,2048]{2,1,0:T(2,128)(2,1)} %copy.153), calls=%async_computation.4 | async-start | bytes 1048576 | tf_op jit(solution)/shard_map/all_to_all | solution.py:202
  173.0 2.7 %fusion.118 = f32[32,512]{1,0:T(8,128)} fusion(bf16[32,2048]{1,0:T(8,128)(2,1)S(1)} %add_convert_fusion.1, bf16[2048,512]{1,0:T(8,128)(2,1)} %param.37), kind=kOutput, calls=%fused_computation.192 | convolution fusion | flops 67108864 | bytes 2293760 | tf_op jit(solution)/shard_map/dot_general | solution.py:211
  175.6 14.8 %all-to-all-done.4 = bf16[64,2,2048]{2,1,0:T(2,128)(2,1)S(1)} async-done(((bf16[64,2,2048]{2,1,0:T(2,128)(2,1)}), bf16[64,2,2048]{2,1,0:T(2,128)(2,1)S(1)}, u32[]{:S(2)}, u32[]{:S(2)}) %all-to-all-start.4) | async-done | bytes 524320 | tf_op jit(solution)/shard_map/all_to_all | solution.py:202
  190.7 1.7 gather_fusion.1
  192.4 1.4 reshape.143
  194.5 3.3 %fusion.117 = (f32[32]{0:T(128)S(1)}, f32[32,2048]{1,0:T(8,128)S(1)}) fusion(f32[32,2048]{1,0:T(8,128)S(1)} %multiply_reduce_fusion, bf16[512,2048]{1,0:T(8,128)(2,1)} %param.39, bf16[32,2048]{1,0:T(8,128)(2,1)S(1)} %add_convert_fusion.1, bf16[2048,512]{1,0:T(8,128)(2,1)} %param.38, f32[32,512]{1,0:T(8,128)} %fusion.118), kind=kOutput, calls=%fused_computation.191 | convolution fusion | flops 134643680 | bytes 4915328 | tf_op jit(solution)/shard_map/dot_general | solution.py:214
  198.0 0.8 add_convert_fusion
  (197 shorter events, 14.6 us)
Async XLA Ops:
  6.5 45.1 %copy-start = (bf16[2,256,2048]{2,1,0:T(8,128)(2,1)S(1)}, bf16[2,256,2048]{2,1,0:T(8,128)(2,1)}, u32[]{:S(2)}) copy-start(bf16[2,256,2048]{2,1,0:T(8,128)(2,1)} %param.29) | copy-start | bytes 6291460
  6.5 8.9 %copy-start.19 = (bf16[2,4,64,64]{3,2,1,0:T(8,128)(2,1)S(1)}, bf16[2,4,64,64]{3,2,1,0:T(8,128)(2,1)}, u32[]{:S(2)}) copy-start(bf16[2,4,64,64]{3,2,1,0:T(8,128)(2,1)} %param.25) | copy-start | bytes 196612
  7.6 7.4 %collective-permute-start = (bf16[3,2,256]{2,0,1:T(4,128)(2,1)S(1)}, bf16[3,2,256]{2,0,1:T(4,128)(2,1)S(1)}, u32[]{:S(2)}, u32[]{:S(2)}) collective-permute-start(bf16[3,2,256]{2,0,1:T(4,128)(2,1)S(1)} %slice.395), channel_id=1, source_target_pairs={{0,4},{4,8},{8,12},{12,16},{16,20},{20,24},{24,28},{28,32},{32,36}... | collective-permute-start | bytes 9224 | tf_op jit(solution)/shard_map/ppermute | solution.py:59
  12.8 2.5 %copy-start.7 = (f32[2,256]{1,0:T(2,128)}, f32[2,256]{1,0:T(2,128)S(1)}, u32[]{:S(2)}) copy-start(f32[2,256]{1,0:T(2,128)S(1)} %get-tuple-element.37) | copy-start | bytes 6148
  12.8 2.5 %copy-start.8 = (f32[2,256]{1,0:T(2,128)}, f32[2,256]{1,0:T(2,128)S(1)}, u32[]{:S(2)}) copy-start(f32[2,256]{1,0:T(2,128)S(1)} %get-tuple-element.38) | copy-start | bytes 6148
  12.8 2.5 %copy-start.9 = (f32[2,256]{1,0:T(2,128)}, f32[2,256]{1,0:T(2,128)S(1)}, u32[]{:S(2)}) copy-start(f32[2,256]{1,0:T(2,128)S(1)} %get-tuple-element.39) | copy-start | bytes 6148
  12.9 2.5 %copy-start.10 = (f32[2,256]{1,0:T(2,128)}, f32[2,256]{1,0:T(2,128)S(1)}, u32[]{:S(2)}) copy-start(f32[2,256]{1,0:T(2,128)S(1)} %get-tuple-element.40) | copy-start | bytes 6148
  15.0 0.9 copy-start.20
  19.6 1.2 copy-start.15
  21.6 24.4 %all-to-all-start = ((f32[64,4,256]{2,1,0:T(4,128)}), f32[64,4,256]{2,1,0:T(4,128)S(1)}, u32[]{:S(2)}, u32[]{:S(2)}) async-start(f32[64,4,256]{2,1,0:T(4,128)} %broadcast_in_dim.61), calls=%async_computation | async-start | bytes 524288 | tf_op jit(solution)/shard_map/all_to_all | solution.py:12
  35.6 12.9 %copy-start.17 = (s32[128]{0:T(128)}, s32[128]{0:T(128)S(1)}, u32[]{:S(2)}) copy-start(s32[128]{0:T(128)S(1)} %fusion.90) | copy-start | bytes 1540
  48.9 1.2 copy-start.5
  50.3 1.2 copy-start.6
  50.8 0.9 copy-start.4
  51.7 5.6 %copy-start.21 = (s32[128]{0:T(128)S(1)}, s32[128]{0:T(128)}, u32[]{:S(2)}) copy-start(s32[128]{0:T(128)} %scatter_custom_fusion) | copy-start | bytes 1540
  51.7 14.7 %copy-start.1 = (bf16[32,2048]{1,0:T(8,128)(2,1)S(1)}, bf16[32,2048]{1,0:T(8,128)(2,1)}, u32[]{:S(2)}) copy-start(bf16[32,2048]{1,0:T(8,128)(2,1)} %param.21) | copy-start | bytes 393220
  53.0 13.8 %copy-start.11 = (f32[2048]{0:T(1024)S(1)}, f32[2048]{0:T(1024)}, u32[]{:S(2)}) copy-start(f32[2048]{0:T(1024)} %param.31) | copy-start | bytes 24580
  53.0 13.8 %copy-start.12 = (f32[2048]{0:T(1024)S(1)}, f32[2048]{0:T(1024)}, u32[]{:S(2)}) copy-start(f32[2048]{0:T(1024)} %param.30) | copy-start | bytes 24580
  53.0 13.3 %all-to-all-start.1 = ((bf16[4,32,2048]{2,1,0:T(8,128)(2,1)}), bf16[4,32,2048]{2,1,0:T(8,128)(2,1)S(1)}, u32[]{:S(2)}, u32[]{:S(2)}) async-start(bf16[4,32,2048]{2,1,0:T(8,128)(2,1)} %bitcast.17), calls=%async_computation.1 | async-start | bytes 1048576 | tf_op jit(solution)/shard_map/all_to_all | solution.py:70
  57.3 65.3 %all-gather.3.cloned.1.call-start = ((), (), s32[]{:S(2)}) async-start(), calls=%async_computation.5 | async-start | bytes 2621440 | tf_op jit(solution)/shard_map/all_gather | solution.py:195
  94.7 30.2 %copy-start.2 = (bf16[1,128,2048]{2,1,0:T(8,128)(2,1)S(1)}, bf16[1,128,2048]{2,1,0:T(8,128)(2,1)}, u32[]{:S(2)}) copy-start(bf16[1,128,2048]{2,1,0:T(8,128)(2,1)} %param.36) | copy-start | bytes 1572868
  94.7 30.2 %copy-start.3 = (bf16[1,2048,128]{2,1,0:T(8,128)(2,1)S(1)}, bf16[1,2048,128]{2,1,0:T(8,128)(2,1)}, u32[]{:S(2)}) copy-start(bf16[1,2048,128]{2,1,0:T(8,128)(2,1)} %param.35) | copy-start | bytes 1572868
  159.2 13.6 %copy-start.16 = (f32[128,4]{0,1:T(4,128)S(1)}, f32[128,4]{0,1:T(4,128)}, u32[]{:S(2)}) copy-start(f32[128,4]{0,1:T(4,128)} %param.33) | copy-start | bytes 6148
  159.2 13.8 %copy-start.18 = (s32[128]{0:T(128)S(1)}, s32[128]{0:T(128)}, u32[]{:S(2)}) copy-start(s32[128]{0:T(128)} %copy-done.17) | copy-start | bytes 1540
  160.9 29.6 %all-to-all-start.4 = ((bf16[64,2,2048]{2,1,0:T(2,128)(2,1)}), bf16[64,2,2048]{2,1,0:T(2,128)(2,1)S(1)}, u32[]{:S(2)}, u32[]{:S(2)}) async-start(bf16[64,2,2048]{2,1,0:T(2,128)(2,1)} %copy.153), calls=%async_computation.4 | async-start | bytes 1048576 | tf_op jit(solution)/shard_map/all_to_all | solution.py:202
  194.5 3.5 %copy-start.13 = (f32[2048]{0:T(1024)S(1)}, f32[2048]{0:T(1024)}, u32[]{:S(2)}) copy-start(f32[2048]{0:T(1024)} %param.41) | copy-start | bytes 24580
  194.5 3.5 %copy-start.14 = (f32[2048]{0:T(1024)S(1)}, f32[2048]{0:T(1024)}, u32[]{:S(2)}) copy-start(f32[2048]{0:T(1024)} %param.40) | copy-start | bytes 24580
Sparse Core Ops, SparseCore 0:
  94.9 27.6 all-gather.2
where the time goes:
time: 207 us; the launch traced here: 206 us
  waiting for transfers between devices  58.8 us (28%)
  blocking collectives  52.1 us (25%)
  starting transfers between devices  32 us (15%)
  local copies, waits for them, and re-layouts  19.8 us (10%)
  matrix products  15.4 us (7%)
  between operations  14.3 us (7%)
  other arithmetic  13.3 us (6%)
    all_to_all x1, blocking collectives, summed_on_arrival(): lax.all_to_all(cut_along(shard, dim, count), axis, 0, 0, tiled=True)  28.9 us
    all_gather x1, waiting for transfers between devices, shards(): fanned = lax.all_gather(arrived[None], 'tp', axis=0, tiled=True)  27.8 us
    all_to_all x1, blocking collectives, shards(): lax.all_to_all(outgoing, 'sp', split_axis=0, concat_axis=0, tiled=True)  23.1 us
    all_to_all x1, waiting for transfers between devices, shards(): lax.all_to_all(leaving, 'sp', split_axis=0, concat_axis=0, tiled=True)  14.8 us
    all_to_all x1, starting transfers between devices, shards(): lax.all_to_all(leaving, 'sp', split_axis=0, concat_axis=0, tiled=True)  11.9 us
    all_to_all x1, starting transfers between devices, copy_for_each(): lax.all_to_all(jnp.broadcast_to(shard[None], (count, *shard.shape)), axis...  11.3 us
    all_to_all x1, waiting for transfers between devices, summed_on_arrival(): lax.all_to_all(cut_along(shard, dim, count), axis, 0, 0, tiled=True)  8.83 us
    all_to_all x1, waiting for transfers between devices, copy_for_each(): lax.all_to_all(jnp.broadcast_to(shard[None], (count, *shard.shape)), axis...  7.34 us
  transfers between devices with their start and end apart: 5, of which 4 were waited for; matrix products, arithmetic and copies ran while one was open for 6% of the time, Pallas kernels for 0%

commit v1 on v0

--- a/solution.py
+++ b/solution.py
@@ -192,7 +192,9 @@
     outgoing = jnp.take(padded_rows, table, axis=0).reshape(expert_count, capacity, width)
     arrived = lax.all_to_all(outgoing, "sp", split_axis=0, concat_axis=0, tiled=True)
     slots = arrived.shape[1]
-    fanned = lax.all_gather(arrived[None], "tp", axis=0, tiled=True)
+    fanned = jnp.concatenate(
+        lax.all_to_all(jnp.stack([arrived[None]] * lax.axis_size("tp")), "tp", 0, 0), axis=0
+    )
     shaped = fanned.reshape(tp_count, -1, local_count, slots, width)
     partial_value = expert_terms(
         shaped, "xslc", routed_gate_weight, routed_up_weight, routed_down_weight

time: 207 us -> 188 us (0.908)
  blocking collectives: 52.1 us -> 80.5 us
  waiting for transfers between devices: 58.8 us -> 31.1 us
  between operations: 14.3 us -> 0.87 us
  starting transfers between devices: 32 us -> 27.2 us
    all_to_all x0 -> x1, blocking collectives: none -> 28.6 us  [shards(): lax.all_to_all(jnp.stack([arrived[None]] * lax.axis_size('tp')), 'tp', 0, 0)]
    all_gather x1 -> x0, waiting for transfers between devices: 27.8 us -> none  [shards(): fanned = lax.all_gather(arrived[None], 'tp', axis=0, tiled=True)]
    all_to_all x1, starting transfers between devices: 11.9 us -> 7.11 us  [shards(): lax.all_to_all(leaving, 'sp', split_axis=0, concat_axis=0, tiled=True)]
  transfers between devices with their start and end apart: 5 -> 4, of which waited for: 4 -> 3; matrix products, arithmetic and copies ran while one was open for 6% -> 6% of each run, Pallas kernels for 0% -> 0%
where the time goes in v1:
time: 188 us; the launch traced here: 187 us
  blocking collectives  80.5 us (43%)
  waiting for transfers between devices  31.1 us (17%)
  starting transfers between devices  27.2 us (14%)
  local copies, waits for them, and re-layouts  20.5 us (11%)
  matrix products  14 us (7%)
  other arithmetic  13.3 us (7%)
    all_to_all x1, blocking collectives, summed_on_arrival(): lax.all_to_all(cut_along(shard, dim, count), axis, 0, 0, tiled=True)  28.8 us
    all_to_all x1, blocking collectives, shards(): lax.all_to_all(jnp.stack([arrived[None]] * lax.axis_size('tp')), 'tp', 0, 0)  28.6 us
    all_to_all x1, blocking collectives, shards(): lax.all_to_all(outgoing, 'sp', split_axis=0, concat_axis=0, tiled=True)  23.1 us
    all_to_all x1, waiting for transfers between devices, shards(): lax.all_to_all(leaving, 'sp', split_axis=0, concat_axis=0, tiled=True)  14.8 us
    all_to_all x1, starting transfers between devices, copy_for_each(): lax.all_to_all(jnp.broadcast_to(shard[None], (count, *shard.shape)), axis...  11.3 us
    all_to_all x1, waiting for transfers between devices, summed_on_arrival(): lax.all_to_all(cut_along(shard, dim, count), axis, 0, 0, tiled=True)  8.84 us
    all_to_all x1, waiting for transfers between devices, copy_for_each(): lax.all_to_all(jnp.broadcast_to(shard[None], (count, *shard.shape)), axis...  7.4 us
    all_to_all x1, starting transfers between devices, shards(): lax.all_to_all(leaving, 'sp', split_axis=0, concat_axis=0, tiled=True)  7.11 us
  transfers between devices with their start and end apart: 4, of which 3 were waited for; matrix products, arithmetic and copies ran while one was open for 6% of the time, Pallas kernels for 0%

profile of v1, /device:TPU:1, one launch (start us, length us, event | category | flops | bytes accessed | tf_op | source)
XLA Modules:
  0.0 187.5 jit_solution(10463653834387888441)
XLA Ops:
  0.0 1.1 copy.122
  1.1 4.5 %collective-permute-start = (bf16[3,2,256]{2,0,1:T(4,128)(2,1)S(1)}, bf16[3,2,256]{2,0,1:T(4,128)(2,1)S(1)}, u32[]{:S(2)}, u32[]{:S(2)}) collective-permute-start(bf16[3,2,256]{2,0,1:T(4,128)(2,1)S(1)} %slice.395), channel_id=1, source_target_pairs={{0,4},{4,8},{8,12},{12,16},{16,20},{20,24},{24,28},{28,32},{32,36}... | collective-permute-start | bytes 9224 | tf_op jit(solution)/shard_map/ppermute | solution.py:59
  7.0 0.8 copy.139
  9.8 1.0 fusion.101
  12.3 0.8 copy.156
  13.1 1.2 fusion.52
  15.1 11.3 %all-to-all-start = ((f32[64,4,256]{2,1,0:T(4,128)}), f32[64,4,256]{2,1,0:T(4,128)S(1)}, u32[]{:S(2)}, u32[]{:S(2)}) async-start(f32[64,4,256]{2,1,0:T(4,128)} %broadcast_in_dim.58), calls=%async_computation | async-start | bytes 524288 | tf_op jit(solution)/shard_map/all_to_all | solution.py:12
  26.4 0.8 fusion.60
  27.5 0.9 select_reduce_fusion
  29.1 1.4 scatter_custom_fusion
  32.1 7.4 %all-to-all-done = f32[64,4,256]{2,1,0:T(4,128)S(1)} async-done(((f32[64,4,256]{2,1,0:T(4,128)}), f32[64,4,256]{2,1,0:T(4,128)S(1)}, u32[]{:S(2)}, u32[]{:S(2)}) %all-to-all-start) | async-done | bytes 262176 | tf_op jit(solution)/shard_map/all_to_all | solution.py:12
  41.1 0.9 fusion.109
  42.5 1.0 fusion.106
  45.2 1.3 fusion.1
  46.5 4.3 %all-to-all-start.1 = ((bf16[4,32,2048]{2,1,0:T(8,128)(2,1)}), bf16[4,32,2048]{2,1,0:T(8,128)(2,1)S(1)}, u32[]{:S(2)}, u32[]{:S(2)}) async-start(bf16[4,32,2048]{2,1,0:T(8,128)(2,1)} %bitcast.17), calls=%async_computation.1 | async-start | bytes 1048576 | tf_op jit(solution)/shard_map/all_to_all | solution.py:70
  51.0 8.8 %all-to-all-done.1 = bf16[4,32,2048]{2,1,0:T(8,128)(2,1)S(1)} async-done(((bf16[4,32,2048]{2,1,0:T(8,128)(2,1)}), bf16[4,32,2048]{2,1,0:T(8,128)(2,1)S(1)}, u32[]{:S(2)}, u32[]{:S(2)}) %all-to-all-start.1) | async-done | bytes 524320 | tf_op jit(solution)/shard_map/all_to_all | solution.py:70
  60.5 0.9 gather_fusion
  61.4 1.1 gather.10
  62.6 1.6 broadcast_select_fusion
  64.2 23.1 %all_to_all.30 = bf16[64,2,2048]{2,1,0:T(2,128)(2,1)S(1)} all-to-all(bf16[64,2,2048]{2,1,0:T(2,128)(2,1)S(1)} %broadcast_select_fusion), channel_id=1, replica_groups=mesh['sp'=64,'tp'=4] {'sp'}, dimensions={0} | all-to-all | bytes 1048576 | tf_op jit(solution)/shard_map/all_to_all | solution.py:193
  87.7 28.6 %all_to_all.31 = bf16[4,1,64,2,2048]{4,2,3,1,0:T(8,128)(2,1)S(1)} all-to-all(bf16[4,1,64,2,2048]{4,2,3,1,0:T(8,128)(2,1)S(1)} %stack.11), channel_id=1, replica_groups=mesh['sp'=64,'tp'=4] {'tp'}, dimensions={0} | all-to-all | bytes 4194304 | tf_op jit(solution)/shard_map/all_to_all | solution.py:196
  116.4 1.3 copy-done.1
  118.4 5.5 %fusion = bf16[4,1,64,1,2,2048]{5,2,4,3,1,0:T(8,128)(2,1)} fusion(bf16[4,1,64,2,2048]{4,2,3,1,0:T(8,128)(2,1)} %copy-done.1, bf16[1,128,2048]{2,1,0:T(8,128)(2,1)} %param.36, bf16[1,2048,128]{2,1,0:T(8,128)(2,1)} %param.35, f32[4,64,1,2,128]{4,1,3,0,2:T(8,128)S(1)} %fusion.7), kind=kOutput, calls=%fused_computation.4 | convolution fusion | flops 538312704 | bytes 5505024 | tf_op jit(solution)/shard_map/xslcf,lfd->xslcd/dot_general | solution.py:104
  123.9 28.8 %all_to_all.32 = bf16[4,1,64,1,2,2048]{5,2,4,3,1,0:T(8,128)(2,1)S(1)} all-to-all(bf16[4,1,64,1,2,2048]{5,2,4,3,1,0:T(8,128)(2,1)} %fusion), channel_id=1, replica_groups=mesh['sp'=64,'tp'=4] {'tp'}, dimensions={0} | all-to-all | bytes 4194304 | tf_op jit(solution)/shard_map/all_to_all | solution.py:70
  153.0 1.3 copy.143
  154.3 7.1 %all-to-all-start.5 = ((bf16[64,2,2048]{2,1,0:T(2,128)(2,1)}), bf16[64,2,2048]{2,1,0:T(2,128)(2,1)S(1)}, u32[]{:S(2)}, u32[]{:S(2)}) async-start(bf16[64,2,2048]{2,1,0:T(2,128)(2,1)} %copy.143), calls=%async_computation.5 | async-start | bytes 1048576 | tf_op jit(solution)/shard_map/all_to_all | solution.py:204
  161.6 2.7 %fusion.118 = f32[32,512]{1,0:T(8,128)} fusion(bf16[32,2048]{1,0:T(8,128)(2,1)S(1)} %add_convert_fusion.1, bf16[2048,512]{1,0:T(8,128)(2,1)} %param.37), kind=kOutput, calls=%fused_computation.192 | convolution fusion | flops 67108864 | bytes 2293760 | tf_op jit(solution)/shard_map/dot_general | solution.py:213
  164.3 14.8 %all-to-all-done.5 = bf16[64,2,2048]{2,1,0:T(2,128)(2,1)S(1)} async-done(((bf16[64,2,2048]{2,1,0:T(2,128)(2,1)}), bf16[64,2,2048]{2,1,0:T(2,128)(2,1)S(1)}, u32[]{:S(2)}, u32[]{:S(2)}) %all-to-all-start.5) | async-done | bytes 524320 | tf_op jit(solution)/shard_map/all_to_all | solution.py:204
  179.3 1.7 gather_fusion.1
  181.1 1.4 reshape.147
  183.2 3.3 %fusion.117 = (f32[32]{0:T(128)S(1)}, f32[32,2048]{1,0:T(8,128)S(1)}) fusion(f32[32,2048]{1,0:T(8,128)S(1)} %multiply_reduce_fusion, bf16[512,2048]{1,0:T(8,128)(2,1)} %param.39, bf16[32,2048]{1,0:T(8,128)(2,1)S(1)} %add_convert_fusion.1, bf16[2048,512]{1,0:T(8,128)(2,1)} %param.38, f32[32,512]{1,0:T(8,128)} %fusion.118), kind=kOutput, calls=%fused_computation.191 | convolution fusion | flops 134643680 | bytes 4915328 | tf_op jit(solution)/shard_map/dot_general | solution.py:216
  186.7 0.8 add_convert_fusion
  (196 shorter events, 15.0 us)
Async XLA Ops:
  0.0 45.2 %copy-start = (bf16[2,256,2048]{2,1,0:T(8,128)(2,1)S(1)}, bf16[2,256,2048]{2,1,0:T(8,128)(2,1)}, u32[]{:S(2)}) copy-start(bf16[2,256,2048]{2,1,0:T(8,128)(2,1)} %param.29) | copy-start | bytes 6291460
  0.0 8.9 %copy-start.19 = (bf16[2,4,64,64]{3,2,1,0:T(8,128)(2,1)S(1)}, bf16[2,4,64,64]{3,2,1,0:T(8,128)(2,1)}, u32[]{:S(2)}) copy-start(bf16[2,4,64,64]{3,2,1,0:T(8,128)(2,1)} %param.25) | copy-start | bytes 196612
  1.1 7.4 %collective-permute-start = (bf16[3,2,256]{2,0,1:T(4,128)(2,1)S(1)}, bf16[3,2,256]{2,0,1:T(4,128)(2,1)S(1)}, u32[]{:S(2)}, u32[]{:S(2)}) collective-permute-start(bf16[3,2,256]{2,0,1:T(4,128)(2,1)S(1)} %slice.395), channel_id=1, source_target_pairs={{0,4},{4,8},{8,12},{12,16},{16,20},{20,24},{24,28},{28,32},{32,36}... | collective-permute-start | bytes 9224 | tf_op jit(solution)/shard_map/ppermute | solution.py:59
  6.3 2.5 %copy-start.7 = (f32[2,256]{1,0:T(2,128)}, f32[2,256]{1,0:T(2,128)S(1)}, u32[]{:S(2)}) copy-start(f32[2,256]{1,0:T(2,128)S(1)} %get-tuple-element.37) | copy-start | bytes 6148
  6.3 2.5 %copy-start.8 = (f32[2,256]{1,0:T(2,128)}, f32[2,256]{1,0:T(2,128)S(1)}, u32[]{:S(2)}) copy-start(f32[2,256]{1,0:T(2,128)S(1)} %get-tuple-element.38) | copy-start | bytes 6148
  6.3 2.5 %copy-start.9 = (f32[2,256]{1,0:T(2,128)}, f32[2,256]{1,0:T(2,128)S(1)}, u32[]{:S(2)}) copy-start(f32[2,256]{1,0:T(2,128)S(1)} %get-tuple-element.39) | copy-start | bytes 6148
  6.3 2.5 %copy-start.10 = (f32[2,256]{1,0:T(2,128)}, f32[2,256]{1,0:T(2,128)S(1)}, u32[]{:S(2)}) copy-start(f32[2,256]{1,0:T(2,128)S(1)} %get-tuple-element.40) | copy-start | bytes 6148
  8.5 0.9 copy-start.20
  13.1 1.2 copy-start.15
  15.1 24.4 %all-to-all-start = ((f32[64,4,256]{2,1,0:T(4,128)}), f32[64,4,256]{2,1,0:T(4,128)S(1)}, u32[]{:S(2)}, u32[]{:S(2)}) async-start(f32[64,4,256]{2,1,0:T(4,128)} %broadcast_in_dim.58), calls=%async_computation | async-start | bytes 524288 | tf_op jit(solution)/shard_map/all_to_all | solution.py:12
  29.1 13.0 %copy-start.17 = (s32[128]{0:T(128)}, s32[128]{0:T(128)S(1)}, u32[]{:S(2)}) copy-start(s32[128]{0:T(128)S(1)} %fusion.90) | copy-start | bytes 1540
  42.4 1.2 copy-start.5
  43.8 1.2 copy-start.6
  44.3 0.9 copy-start.4
  45.2 5.6 %copy-start.21 = (s32[128]{0:T(128)S(1)}, s32[128]{0:T(128)}, u32[]{:S(2)}) copy-start(s32[128]{0:T(128)} %scatter_custom_fusion) | copy-start | bytes 1540
  45.2 14.7 %copy-start.2 = (bf16[32,2048]{1,0:T(8,128)(2,1)S(1)}, bf16[32,2048]{1,0:T(8,128)(2,1)}, u32[]{:S(2)}) copy-start(bf16[32,2048]{1,0:T(8,128)(2,1)} %param.21) | copy-start | bytes 393220
  46.5 13.8 %copy-start.11 = (f32[2048]{0:T(1024)S(1)}, f32[2048]{0:T(1024)}, u32[]{:S(2)}) copy-start(f32[2048]{0:T(1024)} %param.31) | copy-start | bytes 24580
  46.5 13.8 %copy-start.12 = (f32[2048]{0:T(1024)S(1)}, f32[2048]{0:T(1024)}, u32[]{:S(2)}) copy-start(f32[2048]{0:T(1024)} %param.30) | copy-start | bytes 24580
  46.5 13.3 %all-to-all-start.1 = ((bf16[4,32,2048]{2,1,0:T(8,128)(2,1)}), bf16[4,32,2048]{2,1,0:T(8,128)(2,1)S(1)}, u32[]{:S(2)}, u32[]{:S(2)}) async-start(bf16[4,32,2048]{2,1,0:T(8,128)(2,1)} %bitcast.17), calls=%async_computation.1 | async-start | bytes 1048576 | tf_op jit(solution)/shard_map/all_to_all | solution.py:70
  87.7 30.0 %copy-start.3 = (bf16[1,2048,128]{2,1,0:T(8,128)(2,1)S(1)}, bf16[1,2048,128]{2,1,0:T(8,128)(2,1)}, u32[]{:S(2)}) copy-start(bf16[1,2048,128]{2,1,0:T(8,128)(2,1)} %param.34) | copy-start | bytes 1572868
  116.3 1.3 copy-start.1
  152.6 8.8 %copy-start.16 = (f32[128,4]{0,1:T(4,128)S(1)}, f32[128,4]{0,1:T(4,128)}, u32[]{:S(2)}) copy-start(f32[128,4]{0,1:T(4,128)} %param.33) | copy-start | bytes 6148
  152.6 9.0 %copy-start.18 = (s32[128]{0:T(128)S(1)}, s32[128]{0:T(128)}, u32[]{:S(2)}) copy-start(s32[128]{0:T(128)} %copy-done.17) | copy-start | bytes 1540
  154.3 24.8 %all-to-all-start.5 = ((bf16[64,2,2048]{2,1,0:T(2,128)(2,1)}), bf16[64,2,2048]{2,1,0:T(2,128)(2,1)S(1)}, u32[]{:S(2)}, u32[]{:S(2)}) async-start(bf16[64,2,2048]{2,1,0:T(2,128)(2,1)} %copy.143), calls=%async_computation.5 | async-start | bytes 1048576 | tf_op jit(solution)/shard_map/all_to_all | solution.py:204
  183.2 3.5 %copy-start.13 = (f32[2048]{0:T(1024)S(1)}, f32[2048]{0:T(1024)}, u32[]{:S(2)}) copy-start(f32[2048]{0:T(1024)} %param.41) | copy-start | bytes 24580
  183.2 3.5 %copy-start.14 = (f32[2048]{0:T(1024)S(1)}, f32[2048]{0:T(1024)}, u32[]{:S(2)}) copy-start(f32[2048]{0:T(1024)} %param.40) | copy-start | bytes 24580
